TPU v7x, 32 devices: a whole 2x2x4 slice. The times are simulated.
32 devices in a mesh: ep: 4 (over y, x), tp: 8 (over z, core).
Axes of the slice: x: 2, y: 2, z: 4, core: 2. Of those that a mesh axis runs over, the one named last changes fastest.
Arguments:
- hidden_in: bfloat16 [128, 4096], P('ep'), may hold values from -6 to 6
- mix_gain: float32 [4096], replicated, may hold values from 0.1 to 1.9
- w_query: bfloat16 [4096, 2048], P('ep', 'tp'), may hold values from -0.09375 to 0.09375
- w_key: bfloat16 [4096, 2048], P('ep', 'tp'), may hold values from -0.09375 to 0.09375
- w_value: bfloat16 [4096, 2048], P('ep', 'tp'), may hold values from -0.09375 to 0.09375
- w_outgate: bfloat16 [4096, 2048], P('ep', 'tp'), may hold values from -0.09375 to 0.09375
- w_gates: bfloat16 [2, 4096, 32], P(None, None, 'tp'), may hold values from -0.09375 to 0.09375
- gate_bias: float32 [2, 32], P(None, 'tp'), may hold values from -1 to 4
- state_matrix: float32 [128, 32, 64, 64], P('ep', 'tp'), may hold values from -2 to 2
- state_norm: float32 [128, 32, 64], P('ep', 'tp'), may hold values from -2 to 2
- state_max: float32 [128, 32], P('ep', 'tp'), may hold values from -3 to 3
- w_mix_out: bfloat16 [2048, 4096], P('tp'), may hold values from -0.125 to 0.125
- ffn_gain: float32 [4096], replicated, may hold values from 0.1 to 1.9
- routes: int32 [128, 2], replicated, may hold values from 0 to 7, all different within a row; in each aligned block of 32 rows (0 to 31, 32 to 63, ...) at most 9 rows name the same one
- route_weights: float32 [128, 2], P('ep'), may hold values from 0.1 to 1
- expert_gate: bfloat16 [8, 4096, 2048], P('ep', None, 'tp'), may hold values from -0.09375 to 0.09375
- expert_up: bfloat16 [8, 4096, 2048], P('ep', None, 'tp'), may hold values from -0.09375 to 0.09375
- expert_down: bfloat16 [8, 2048, 4096], P('ep', 'tp'), may hold values from -0.125 to 0.125
- shared_gate: bfloat16 [4096, 1024], P(None, 'tp'), may hold values from -0.09375 to 0.09375
- shared_up: bfloat16 [4096, 1024], P(None, 'tp'), may hold values from -0.09375 to 0.09375
- shared_down: bfloat16 [1024, 4096], P('tp'), may hold values from -0.1875 to 0.1875
Outputs:
- result: bfloat16 [128, 4096], P('ep', 'tp')
- new_matrix: float32 [128, 32, 64, 64], P('ep', 'tp')
- new_norm: float32 [128, 32, 64], P('ep', 'tp')
- new_max: float32 [128, 32], P('ep', 'tp')
Inputs may be any that keep to these rules, and one draw needn't show every extreme that they name: `routes`: each row names 2 different experts. In each aligned block of 32 rows (the rows of one device group along ep) no expert is named by more than 9 rows, a bound that some block reaches.
All inputs are finite; a program needn't handle non-finite values.
Results may differ from a plain program's by a relative error of at most 0.023.
Values may be sent and summed in bfloat16 or wider, within the bound.
No kernel may reach another device: no remote copies, remote signals or barrier semaphores. Data moves between devices by JAX's collectives and lax.ppermute only.
A program may use at most 64 MiB of HBM per device.

v0:
```python
import jax
import jax.numpy as jnp
from jax import lax
from jax.sharding import PartitionSpec as P

norm_eps = 1e-06


def rms_scale(inputs, scales):
    floats = inputs.astype(jnp.float32)
    return floats * lax.rsqrt(jnp.mean(floats * floats, -1, keepdims=True) + norm_eps) * scales


def slot_ranks(chosen, experts):
    flat_ids = chosen.reshape(-1)
    onehot = (flat_ids[:, None] == jnp.arange(experts, dtype=jnp.int32)[None, :]).astype(jnp.int32)
    earlier = jnp.cumsum(onehot, 0) - onehot
    return jnp.sum(earlier * onehot, 1).reshape(chosen.shape)


def per_device(
    hidden_in,
    mix_gain,
    w_query,
    w_key,
    w_value,
    w_outgate,
    w_gates,
    gate_bias,
    state_matrix,
    state_norm,
    state_max,
    w_mix_out,
    ffn_gain,
    routes,
    route_weights,
    expert_gate,
    expert_up,
    expert_down,
    shared_gate,
    shared_up,
    shared_down,
):
    ep_count = lax.axis_size("ep")
    tp_count = lax.axis_size("tp")
    group_index = lax.axis_index("ep")
    column_index = lax.axis_index("tp")
    seq_rows, width = hidden_in.shape
    heads_dev = state_matrix.shape[1]
    head_dim = state_matrix.shape[2]
    top_count = routes.shape[1]
    local_experts = expert_gate.shape[0]
    expert_total = local_experts * ep_count
    capacity = max(2, seq_rows * top_count // expert_total + 1)
    slot_count = ep_count * capacity
    slice_width = width // tp_count
    normed = rms_scale(hidden_in, mix_gain).astype(jnp.bfloat16)
    gathered = lax.all_to_all(normed, "ep", split_axis=1, concat_axis=0, tiled=True)
    joined = jnp.concatenate([w_query, w_key, w_value, w_outgate], 1)
    projected = lax.psum_scatter(
        jnp.dot(gathered, joined, preferred_element_type=jnp.float32).astype(jnp.bfloat16),
        "ep",
        scatter_dimension=0,
        tiled=True,
    )
    head_cols = heads_dev * head_dim

    def heads_of(role_index):
        part = projected[:, role_index * head_cols : (role_index + 1) * head_cols]
        return part.astype(jnp.float32).reshape(seq_rows, heads_dev, head_dim)

    query_heads = heads_of(0)
    key_heads = heads_of(1) * head_dim ** (-0.5)
    value_heads = heads_of(2)
    out_gate = heads_of(3)
    gate_pre = jnp.einsum("sd,gdh->gsh", normed, w_gates, preferred_element_type=jnp.float32)
    gate_pre = gate_pre + gate_bias[:, None, :]
    carried = jax.nn.log_sigmoid(gate_pre[1]) + state_max
    new_max = jnp.maximum(carried, gate_pre[0])
    forget_weight = jnp.exp(carried - new_max)[..., None]
    input_weight = jnp.exp(gate_pre[0] - new_max)[..., None]
    new_norm = forget_weight * state_norm + input_weight * key_heads
    new_matrix = (
        forget_weight[..., None] * state_matrix
        + (input_weight * value_heads)[..., :, None] * key_heads[..., None, :]
    )
    numerator = jnp.einsum(
        "shek,shk->she", new_matrix, query_heads, precision=lax.Precision.HIGHEST
    )
    denominator = jnp.maximum(jnp.abs(jnp.sum(new_norm * query_heads, -1)), 1.0)
    gated_out = (jax.nn.sigmoid(out_gate) * numerator / denominator[..., None]).reshape(
        seq_rows, head_cols
    )
    gated_out = gated_out.astype(jnp.bfloat16)
    mixed_part = jnp.dot(gated_out, w_mix_out, preferred_element_type=jnp.float32)
    mixed_own = lax.psum_scatter(
        mixed_part.astype(jnp.bfloat16), "tp", scatter_dimension=1, tiled=True
    ).astype(jnp.float32)
    residual_own = lax.dynamic_slice_in_dim(hidden_in, column_index * slice_width, slice_width, 1)
    stream_own = (residual_own.astype(jnp.float32) + mixed_own).astype(jnp.bfloat16)
    stream = lax.all_gather(stream_own, "tp", axis=1, tiled=True)
    ffn_in = rms_scale(stream, ffn_gain).astype(jnp.bfloat16)
    shared_hidden = (
        jax.nn.silu(jnp.dot(ffn_in, shared_gate, preferred_element_type=jnp.float32))
        * jnp.dot(ffn_in, shared_up, preferred_element_type=jnp.float32)
    ).astype(jnp.bfloat16)
    shared_part = jnp.dot(shared_hidden, shared_down, preferred_element_type=jnp.float32)
    own_routes = lax.dynamic_slice_in_dim(routes, group_index * seq_rows, seq_rows, 0)
    slot_ids = own_routes * capacity + slot_ranks(own_routes, expert_total)
    slot_range = jnp.arange(expert_total * capacity, dtype=jnp.int32)
    matches = slot_ids[:, :, None] == slot_range[None, None, :]
    chooser = jnp.any(matches, 1).astype(jnp.bfloat16)
    outgoing = jnp.einsum("sj,sd->jd", chooser, ffn_in, preferred_element_type=jnp.float32)
    outgoing = outgoing.astype(jnp.bfloat16).reshape(expert_total, capacity, width)
    arrived = lax.all_to_all(outgoing, "ep", split_axis=0, concat_axis=1, tiled=True)
    gate_values = jnp.einsum(
        "erd,edf->erf", arrived, expert_gate, preferred_element_type=jnp.float32
    )
    up_values = jnp.einsum("erd,edf->erf", arrived, expert_up, preferred_element_type=jnp.float32)
    expert_hidden = (jax.nn.silu(gate_values) * up_values).astype(jnp.bfloat16)
    expert_part = jnp.einsum(
        "erf,efd->erd", expert_hidden, expert_down, preferred_element_type=jnp.float32
    )
    expert_part = expert_part.reshape(local_experts * slot_count, width)
    routed_sum, shared_sum = (
        lax.psum_scatter(
            expert_part.astype(jnp.bfloat16), "tp", scatter_dimension=1, tiled=True
        ).astype(jnp.float32),
        lax.psum_scatter(
            shared_part.astype(jnp.bfloat16), "tp", scatter_dimension=1, tiled=True
        ).astype(jnp.float32),
    )
    expert_rows = routed_sum.astype(jnp.bfloat16)
    returned = lax.all_to_all(
        expert_rows.reshape(local_experts, slot_count, slice_width),
        "ep",
        split_axis=1,
        concat_axis=0,
        tiled=True,
    )
    returned = returned.reshape(expert_total * capacity, slice_width)
    weights = jnp.sum(jnp.where(matches, route_weights[:, :, None], 0.0), 1)
    routed = jnp.dot(weights, returned.astype(jnp.float32), precision=lax.Precision.HIGHEST)
    result = (stream_own.astype(jnp.float32) + shared_sum + routed).astype(jnp.bfloat16)
    return (result, new_matrix, new_norm, new_max)


def solution(mesh):
    placed = (
        P("ep", None),
        P(),
        P("ep", "tp"),
        P("ep", "tp"),
        P("ep", "tp"),
        P("ep", "tp"),
        P(None, None, "tp"),
        P(None, "tp"),
        P("ep", "tp", None, None),
        P("ep", "tp", None),
        P("ep", "tp"),
        P("tp", None),
        P(),
        P(),
        P("ep", None),
        P("ep", None, "tp"),
        P("ep", None, "tp"),
        P("ep", "tp", None),
        P(None, "tp"),
        P(None, "tp"),
        P("tp", None),
    )
    return jax.shard_map(
        per_device,
        mesh=mesh,
        in_specs=placed,
        out_specs=(P("ep", "tp"), P("ep", "tp", None, None), P("ep", "tp", None), P("ep", "tp")),
        check_vma=False,
    )
```

profile of v0, /device:TPU:0, one launch (start us, length us, event | category | flops | bytes accessed | tf_op | source)
XLA Modules:
  0.0 207.5 jit_solution(7990342096338553955)
XLA Ops:
  7.2 0.0 copy-start
  7.2 1.3 fusion.19
  8.4 1.1 fusion.21
  9.5 0.7 copy.88
  10.3 5.2 %all-to-all-start = ((bf16[32,4,1024]{2,0,1:T(8,128)(2,1)}), bf16[32,4,1024]{2,0,1:T(8,128)(2,1)S(1)}, u32[]{:S(2)}, u32[]{:S(2)}) async-start(bf16[32,4,1024]{2,0,1:T(8,128)(2,1)} %bitcast.53), calls=%async_computation | async-start | bytes 524288 | tf_op jit(solution)/shard_map/all_to_all | solution.py:58
  15.5 1.0 fusion.14
  16.5 4.3 %all-to-all-done = bf16[32,4,1024]{2,0,1:T(8,128)(2,1)S(1)} async-done(((bf16[32,4,1024]{2,0,1:T(8,128)(2,1)}), bf16[32,4,1024]{2,0,1:T(8,128)(2,1)S(1)}, u32[]{:S(2)}, u32[]{:S(2)}) %all-to-all-start) | async-done | bytes 262176 | tf_op jit(solution)/shard_map/all_to_all | solution.py:58
  20.8 2.7 %fusion.8 = bf16[128,1024]{1,0:T(8,128)(2,1)} fusion(bf16[128,1024]{1,0:T(8,128)(2,1)S(1)} %bitcast.60, bf16[1024,256]{1,0:T(8,128)(2,1)} %param.26, bf16[1024,256]{1,0:T(8,128)(2,1)} %param.25, bf16[1024,256]{1,0:T(8,128)(2,1)} %param.24, bf16[1024,256]{1,0:T(8,128)(2,1)} %param.23), kind=kOutput, calls=%fused_computation.13 | convolution fusion | flops 276955136 | bytes 2621440 | tf_op jit(solution)/shard_map/dot_general | solution.py:61
  23.5 0.0 reduce-scatter.5.cloned.1.call-update
  23.6 0.0 reduce-scatter.7.cloned.1.call-start
  23.6 0.0 copy-start.5
  23.7 0.1 copy.67
  23.8 0.1 copy.68
  23.8 0.1 copy.70
  23.9 0.1 constant_dynamic-slice_fusion
  24.0 0.1 copy.80
  24.1 0.1 eq.28
  24.2 23.9 %reduce-scatter.5.cloned.1.call-done = bf16[32,1024]{1,0:T(8,128)(2,1)} async-done(((bf16[128,1024]{1,0:T(8,128)(2,1)}), bf16[32,1024]{1,0:T(8,128)(2,1)}) %reduce-scatter.5.cloned.1.call-update) | async-done | bytes 65552 | tf_op jit(solution)/shard_map/reduce_scatter | solution.py:60
  48.1 0.8 fusion.54
  48.9 0.1 reshape.97
  49.0 0.1 reshape.111
  49.1 0.1 reshape.104
  49.2 0.1 reshape.106
  49.3 0.8 multiply_reduce_fusion
  50.1 0.7 add_divide_fusion
  50.8 0.1 div.30
  50.9 3.7 %multiply_add_fusion = f32[32,4,64,64]{3,2,1,0:T(8,128)S(1)} fusion(f32[32,4,64,64]{3,2,1,0:T(8,128)} %param.29, f32[32,4,64]{2,1,0:T(4,128)S(1)} %get-tuple-element.9, f32[32,4,64]{2,1,0:T(4,128)S(1)} %get-tuple-element.13, f32[32,4]{1,0:T(8,128)S(1)} %copy.67), kind=kLoop, calls=%fused_computation.4 | loop fusion | flops 1572864 | bytes 4260352 | tf_op jit(solution)/shard_map/add | solution.py:84
  54.7 2.0 copy-done.1
  56.7 3.4 %fusion.55 = f32[32,4,1,64]{3,2,1,0:T(1,128)S(1)} fusion(f32[32,4,64,64]{3,2,1,0:T(8,128)S(1)} %multiply_add_fusion, bf16[32,4,64,1]{2,3,1,0:T(2,128)(2,1)S(1)} %reshape.111), kind=kOutput, calls=%fused_computation.85 | convolution fusion | flops 6291456 | bytes 2146304 | tf_op jit(solution)/shard_map/shek,shk->she/dot_general | solution.py:87
  60.0 0.1 fusion.31
  60.1 0.1 convert_element_type.79
  60.3 1.2 convolution_convert_fusion.3
  61.4 0.0 reduce-scatter.7.cloned.1.call-update
  61.4 0.0 reduce-scatter.11.cloned.1.call-start
  61.5 0.1 fusion.34
  61.6 0.1 reduce_window_sum.11
  61.7 0.2 select_reduce_fusion.1
  61.8 0.1 reshape.99
  62.0 0.1 copy.72
  62.0 0.1 fusion.33
  62.1 30.2 %reduce-scatter.7.cloned.1.call-done = bf16[32,512]{1,0:T(8,128)(2,1)} async-done(((bf16[32,4096]{1,0:T(8,128)(2,1)}), bf16[32,512]{1,0:T(8,128)(2,1)}) %reduce-scatter.7.cloned.1.call-update) | async-done | bytes 32784 | tf_op jit(solution)/shard_map/reduce_scatter | solution.py:96
  92.3 0.8 add_convert_fusion
  93.1 14.2 %all_gather.3 = bf16[32,4096]{1,0:T(8,128)(2,1)S(1)} all-gather(bf16[32,512]{1,0:T(8,128)(2,1)S(1)} %add_convert_fusion), channel_id=1, replica_groups=mesh['ep'=4,'tp'=8] {'tp'}, dimensions={1}, use_global_device_ids=true | all-gather | bytes 294912 | tf_op jit(solution)/shard_map/all_gather | solution.py:101
  107.3 0.2 fusion.22
  107.5 1.2 convolution_convert_fusion.1
  108.7 1.3 reshape.100
  110.0 18.2 %all_to_all.52 = bf16[8,9,4096]{2,1,0:T(8,128)(2,1)S(1)} all-to-all(bf16[8,9,4096]{2,1,0:T(8,128)(2,1)S(1)} %reshape.100), channel_id=1, replica_groups=mesh['ep'=4,'tp'=8] {'ep'}, dimensions={0} | all-to-all | bytes 1179648 | tf_op jit(solution)/shard_map/all_to_all | solution.py:115
  128.2 0.6 copy.73
  128.8 3.1 %fusion.17 = f32[2,36,256]{2,1,0:T(8,128)S(1)} fusion(bf16[2,4096,256]{2,1,0:T(8,128)(2,1)} %param.36, bf16[2,36,4096]{2,0,1:T(2,128)(2,1)S(1)} %bitcast.54), kind=kOutput, calls=%fused_computation.27 | convolution fusion | flops 150994944 | bytes 4857856 | tf_op jit(solution)/shard_map/erd,edf->erf/dot_general | solution.py:116
  131.9 6.0 %convolution_convert_fusion = bf16[2,36,4096]{2,1,0:T(8,128)(2,1)} fusion(bf16[2,256,4096]{2,1,0:T(8,128)(2,1)} %param.38, bf16[2,4096,256]{2,1,0:T(8,128)(2,1)} %param.37, bf16[2,36,4096]{2,0,1:T(2,128)(2,1)S(1)} %bitcast.55, f32[2,36,256]{2,1,0:T(8,128)S(1)} %fusion.17), kind=kOutput, calls=%fused_computation | convolution fusion | flops 302395392 | bytes 9641984 | tf_op jit(solution)/shard_map/erf,efd->erd/dot_general | solution.py:121
  137.9 2.0 convert_element_type.93
  140.0 0.0 reduce-scatter.11.cloned.1.call-update
  140.0 0.0 reduce-scatter.9.cloned.1.call-start
  140.0 1.6 fusion.51
  141.6 2.9 %convolution_convert_fusion.2 = bf16[32,4096]{1,0:T(8,128)(2,1)} fusion(bf16[128,4096]{1,0:T(8,128)(2,1)} %param.41, bf16[4096,128]{1,0:T(8,128)(2,1)} %param.40, f32[32,128]{1,0:T(8,128)S(1)} %fusion.51, bf16[32,4096]{1,0:T(8,128)(2,1)S(1)} %all_gather.3, f32[4096]{0:T(1024)S(1)} %copy-done.2, f32[32]{0:T(128)S(1)} %add_rsqrt_fusion), kind=kOutput, calls=%fused_computation.2 | convolution fusion | flops 67788800 | bytes 2654336 | tf_op jit(solution)/shard_map/dot_general | solution.py:107
  144.5 0.0 reduce-scatter.9.cloned.1.call-update
  144.5 23.9 %reduce-scatter.11.cloned.1.call-done = bf16[72,512]{1,0:T(8,128)(2,1)} async-done(((bf16[72,4096]{1,0:T(8,128)(2,1)}), bf16[72,512]{1,0:T(8,128)(2,1)}) %reduce-scatter.11.cloned.1.call-update) | async-done | bytes 73744 | tf_op jit(solution)/shard_map/reduce_scatter | solution.py:126
  168.4 0.9 reshape.101
  169.3 0.7 copy.76
  170.0 3.6 %all-to-all-start.2 = ((bf16[2,36,512]{2,0,1:T(2,128)(2,1)}), bf16[2,36,512]{2,0,1:T(2,128)(2,1)S(1)}, u32[]{:S(2)}, u32[]{:S(2)}) async-start(bf16[2,36,512]{2,0,1:T(2,128)(2,1)} %copy.76), calls=%async_computation.6 | async-start | bytes 147456 | tf_op jit(solution)/shard_map/all_to_all | solution.py:134
  173.6 0.1 select_reduce_fusion
  173.7 4.8 %all-to-all-done.2 = bf16[2,36,512]{2,0,1:T(2,128)(2,1)S(1)} async-done(((bf16[2,36,512]{2,0,1:T(2,128)(2,1)}), bf16[2,36,512]{2,0,1:T(2,128)(2,1)S(1)}, u32[]{:S(2)}, u32[]{:S(2)}) %all-to-all-start.2) | async-done | bytes 73760 | tf_op jit(solution)/shard_map/all_to_all | solution.py:134
  178.5 20.9 %reduce-scatter.9.cloned.1.call-done = bf16[32,512]{1,0:T(8,128)(2,1)} async-done(((bf16[32,4096]{1,0:T(8,128)(2,1)}), bf16[32,512]{1,0:T(8,128)(2,1)}) %reduce-scatter.9.cloned.1.call-update) | async-done | bytes 32784 | tf_op jit(solution)/shard_map/reduce_scatter | solution.py:129
  199.4 1.5 fusion.12
  (22 shorter events, 0.2 us)
Async XLA Ops:
  7.2 53.1 %copy-start = (bf16[256,4096]{1,0:T(8,128)(2,1)S(1)}, bf16[256,4096]{1,0:T(8,128)(2,1)}, u32[]{:S(2)}) copy-start(bf16[256,4096]{1,0:T(8,128)(2,1)} %param.32) | copy-start | bytes 6291460
  10.3 10.6 %all-to-all-start = ((bf16[32,4,1024]{2,0,1:T(8,128)(2,1)}), bf16[32,4,1024]{2,0,1:T(8,128)(2,1)S(1)}, u32[]{:S(2)}, u32[]{:S(2)}) async-start(bf16[32,4,1024]{2,0,1:T(8,128)(2,1)} %bitcast.53), calls=%async_computation | async-start | bytes 524288 | tf_op jit(solution)/shard_map/all_to_all | solution.py:58
  15.5 32.7 %reduce-scatter.5.cloned.1.call-start = ((), (), s32[]{:S(2)}) async-start(), calls=%async_computation.7 | async-start | bytes 327680 | tf_op jit(solution)/shard_map/reduce_scatter | solution.py:60
  16.5 7.1 %copy-start.4 = (f32[32,4]{0,1:T(4,128)S(1)}, f32[32,4]{0,1:T(4,128)}, u32[]{:S(2)}) copy-start(f32[32,4]{0,1:T(4,128)} %param.31) | copy-start | bytes 1540
  20.8 3.1 %copy-start.7 = (s32[128,2]{0,1:T(2,128)S(1)}, s32[128,2]{0,1:T(2,128)}, u32[]{:S(2)}) copy-start(s32[128,2]{0,1:T(2,128)} %param.34) | copy-start | bytes 3076
  20.8 28.4 %copy-start.3 = (f32[32,4,64]{2,1,0:T(4,128)S(1)}, f32[32,4,64]{2,1,0:T(4,128)}, u32[]{:S(2)}) copy-start(f32[32,4,64]{2,1,0:T(4,128)} %param.30) | copy-start | bytes 98308
  23.6 68.8 %reduce-scatter.7.cloned.1.call-start = ((), (), s32[]{:S(2)}) async-start(), calls=%async_computation.8 | async-start | bytes 294912 | tf_op jit(solution)/shard_map/reduce_scatter | solution.py:96
  23.6 31.0 %copy-start.5 = (f32[32,4]{0,1:T(4,128)}, f32[32,4]{0,1:T(4,128)S(1)}, u32[]{:S(2)}) copy-start(f32[32,4]{0,1:T(4,128)S(1)} %get-tuple-element.8) | copy-start | bytes 1540
  54.6 2.0 copy-start.1
  56.7 50.8 %copy-start.2 = (f32[4096]{0:T(1024)S(1)}, f32[4096]{0:T(1024)}, u32[]{:S(2)}) copy-start(f32[4096]{0:T(1024)} %param.33) | copy-start | bytes 49156
  61.4 106.9 %reduce-scatter.11.cloned.1.call-start = ((), (), s32[]{:S(2)}) async-start(), calls=%async_computation.10 | async-start | bytes 663552 | tf_op jit(solution)/shard_map/reduce_scatter | solution.py:126
  137.9 35.7 %copy-start.6 = (f32[32,2]{0,1:T(2,128)S(1)}, f32[32,2]{0,1:T(2,128)}, u32[]{:S(2)}) copy-start(f32[32,2]{0,1:T(2,128)} %param.35) | copy-start | bytes 772
  140.0 59.4 %reduce-scatter.9.cloned.1.call-start = ((), (), s32[]{:S(2)}) async-start(), calls=%async_computation.9 | async-start | bytes 294912 | tf_op jit(solution)/shard_map/reduce_scatter | solution.py:129
  170.0 8.5 %all-to-all-start.2 = ((bf16[2,36,512]{2,0,1:T(2,128)(2,1)}), bf16[2,36,512]{2,0,1:T(2,128)(2,1)S(1)}, u32[]{:S(2)}, u32[]{:S(2)}) async-start(bf16[2,36,512]{2,0,1:T(2,128)(2,1)} %copy.76), calls=%async_computation.6 | async-start | bytes 147456 | tf_op jit(solution)/shard_map/all_to_all | solution.py:134
Sparse Core Ops, SparseCore 0:
  23.7 24.3 reduce-scatter.4
  61.6 30.7 reduce-scatter.6
  140.1 28.2 reduce-scatter.10
  170.5 28.9 reduce-scatter.8
where the time goes:
time: 208 us
  waiting for transfers between devices  108 us (52%)
  blocking collectives  32.4 us (16%)
  matrix products  24.5 us (12%)
  between operations  14 us (7%)
  other arithmetic  10 us (5%)
  local copies, waits for them, and re-layouts  9.69 us (5%)
  starting transfers between devices  8.96 us (4%)
    reduce_scatter x1, waiting for transfers between devices, per_device(): lax.psum_scatter(mixed_part.astype(jnp.bfloat16), 'tp', scatter_dimension...  30.2 us
    reduce_scatter x1, waiting for transfers between devices, per_device(): lax.psum_scatter(jnp.dot(gathered, joined, preferred_element_type=jnp.flo...  23.9 us
    reduce_scatter x1, waiting for transfers between devices, per_device(): lax.psum_scatter(expert_part.astype(jnp.bfloat16), 'tp', scatter_dimensio...  23.9 us
    reduce_scatter x1, waiting for transfers between devices, per_device(): lax.psum_scatter(shared_part.astype(jnp.bfloat16), 'tp', scatter_dimensio...  20.9 us
    all_to_all x1, blocking collectives, per_device(): lax.all_to_all(outgoing, 'ep', split_axis=0, concat_axis=1, tiled=True)  18.2 us
    all_gather x1, blocking collectives, per_device(): stream = lax.all_gather(stream_own, 'tp', axis=1, tiled=True)  14.2 us
    dot_general x1, matrix products, per_device(): jnp.einsum('erf,efd->erd', expert_hidden, expert_down, preferred_element_...  6.02 us
    all_to_all x1, starting transfers between devices, per_device(): lax.all_to_all(normed, 'ep', split_axis=1, concat_axis=0, tiled=True)  5.19 us
  transfers between devices with their start and end apart: 6, of which 6 were waited for; matrix products, arithmetic and copies ran while one was open for 4% of the time, Pallas kernels for 0%

commit v1 on v0

v1 whole, which is shorter than its diff:
```python
import functools

import jax
import jax.numpy as jnp
from jax import lax
from jax.experimental import pallas as pl
from jax.experimental.pallas import tpu as pltpu
from jax.sharding import PartitionSpec as P

norm_eps = 1e-06


def rms_scale(inputs, scales):
    floats = inputs.astype(jnp.float32)
    return floats * lax.rsqrt(jnp.mean(floats * floats, -1, keepdims=True) + norm_eps) * scales


def swapped(block, axis, distance):
    count = lax.axis_size(axis)
    return lax.ppermute(block, axis, [(source, source ^ distance) for source in range(count)])


def columns_at(array, index, width):
    return lax.dynamic_slice_in_dim(array, index * width, width, 1)


def wide(array):
    return array.astype(jnp.float32)


def feed_forward(core_index, tokens, weights, slice_width, capacity):
    own_half, rows_half, gain = tokens[0], tokens[2], tokens[4]
    expert_gate, shared_gate = weights[0], weights[3]
    experts, width, hidden = expert_gate.shape
    shared_hidden = shared_gate.shape[1]
    own_count, routed_count = own_half.shape[0], rows_half.shape[0]
    row_count = own_count + routed_count
    half_width = width // 2
    chips = half_width // slice_width
    chunks = 4
    depth = width // chunks
    f32, bf16 = jnp.float32, jnp.bfloat16

    def kernel(
        core, own, own_other, routed, routed_other, gain,
        gate_far, up_far, down_far, sgate_far, sup_far, sdown_far,
        mine, theirs,
        gate, up, down, sgate, sup, sdown, inputs, sems,
    ):
        copies = []

        def fetch(source, target):
            copy = pltpu.make_async_copy(source, target, sems.at[len(copies)])
            copy.start()
            copies.append(copy)
            return copy

        chunk_copies = []
        for chunk in range(chunks):
            part = pl.ds(chunk * depth, depth)
            group = []
            for expert in range(experts):
                group.append(fetch(gate_far.at[expert, part], gate.at[expert, part]))
                group.append(fetch(up_far.at[expert, part], up.at[expert, part]))
            group.append(fetch(sgate_far.at[part], sgate.at[part]))
            group.append(fetch(sup_far.at[part], sup.at[part]))
            chunk_copies.append(group)
        down_copies = [fetch(down_far.at[expert], down.at[expert]) for expert in range(experts)]
        down_copies.append(fetch(sdown_far, sdown))

        first_core = core[0] == 0
        for first, other, start in ((own, own_other, 0), (routed, routed_other, own_count)):
            rows = first.shape[0]
            mass = jnp.zeros((rows, 1), f32)
            for chip in range(chips):
                columns = pl.ds(chip * slice_width, slice_width)
                for part in (first, other):
                    value = part[:, columns].astype(f32)
                    mass = mass + jnp.sum(value * value, -1, keepdims=True)
            scale = lax.rsqrt(mass / width + norm_eps)
            for chip in range(chips):
                columns = pl.ds(chip * slice_width, slice_width)
                one, two = first[:, columns].astype(f32), other[:, columns].astype(f32)
                pair = (jnp.where(first_core, one, two), jnp.where(first_core, two, one))
                for parity in range(2):
                    place = pl.ds((2 * chip + parity) * slice_width, slice_width)
                    fed = pair[parity] * scale * gain[:, place]
                    inputs[pl.ds(start, rows), place] = fed.astype(bf16)

        dot = functools.partial(jnp.dot, preferred_element_type=f32)
        gates = [jnp.zeros((routed_count, hidden), f32) for _ in range(experts)]
        ups = [jnp.zeros((routed_count, hidden), f32) for _ in range(experts)]
        own_gate = jnp.zeros((own_count, shared_hidden), f32)
        own_up = jnp.zeros((own_count, shared_hidden), f32)
        for chunk in range(chunks):
            part = pl.ds(chunk * depth, depth)
            for copy in chunk_copies[chunk]:
                copy.wait()
            routed_rows = inputs[pl.ds(own_count, routed_count), part]
            own_rows = inputs[pl.ds(0, own_count), part]
            for expert in range(experts):
                gates[expert] += dot(routed_rows, gate[expert, part, :])
                ups[expert] += dot(routed_rows, up[expert, part, :])
            own_gate += dot(own_rows, sgate[part, :])
            own_up += dot(own_rows, sup[part, :])
        row_ids = lax.broadcasted_iota(jnp.int32, (routed_count, hidden), 0)
        row_expert = row_ids % (experts * capacity) // capacity
        hiddens = []
        for expert in range(experts):
            value = gates[expert] / (1.0 + jnp.exp(-gates[expert])) * ups[expert]
            hiddens.append(jnp.where(row_expert == expert, value, 0.0).astype(bf16))
        own_hidden = (own_gate / (1.0 + jnp.exp(-own_gate)) * own_up).astype(bf16)
        for copy in down_copies:
            copy.wait()
        for chip in range(chips):
            pair = []
            for parity in range(2):
                place = pl.ds((2 * chip + parity) * slice_width, slice_width)
                total = dot(hiddens[0], down[0, :, place])
                for expert in range(1, experts):
                    total = total + dot(hiddens[expert], down[expert, :, place])
                pair.append((dot(own_hidden, sdown[:, place]), total))
            columns = pl.ds(chip * slice_width, slice_width)
            for index, start, rows in ((0, 0, own_count), (1, own_count, routed_count)):
                one, two = pair[0][index], pair[1][index]
                spot = pl.ds(start, rows)
                mine[spot, columns] = jnp.where(first_core, one, two).astype(bf16)
                theirs[spot, columns] = jnp.where(first_core, two, one).astype(bf16)

    near = pl.BlockSpec(memory_space=pltpu.VMEM)
    far = pl.BlockSpec(memory_space=pl.ANY)
    out = jax.ShapeDtypeStruct((row_count, half_width), bf16)
    copies = chunks * (2 * experts + 2) + experts + 1
    scratch = [pltpu.VMEM(weight.shape, bf16) for weight in weights]
    scratch += [pltpu.VMEM((row_count, width), bf16), pltpu.SemaphoreType.DMA((copies,))]
    return pl.pallas_call(
        kernel,
        out_shape=(out, out),
        in_specs=[pl.BlockSpec(memory_space=pltpu.SMEM)] + [near] * 5 + [far] * 6,
        out_specs=(near, near),
        scratch_shapes=scratch,
        compiler_params=pltpu.CompilerParams(vmem_limit_bytes=58 * 1024 * 1024),
        name="feed_forward",
    )(core_index, *tokens, *weights)


def per_device(
    hidden_in,
    mix_gain,
    w_query,
    w_key,
    w_value,
    w_outgate,
    w_gates,
    gate_bias,
    state_matrix,
    state_norm,
    state_max,
    w_mix_out,
    ffn_gain,
    routes,
    route_weights,
    expert_gate,
    expert_up,
    expert_down,
    shared_gate,
    shared_up,
    shared_down,
):
    ep_count = lax.axis_size("ep")
    tp_count = lax.axis_size("tp")
    group_index = lax.axis_index("ep")
    column_index = lax.axis_index("tp")
    core_index = column_index % 2
    chip_index = column_index // 2
    chip_count = tp_count // 2
    seq_rows, width = hidden_in.shape
    heads_dev = state_matrix.shape[1]
    head_dim = state_matrix.shape[2]
    top_count = routes.shape[1]
    local_experts = expert_gate.shape[0]
    expert_total = local_experts * ep_count
    capacity = max(2, seq_rows * top_count // expert_total + 1)
    group_slots = local_experts * capacity
    slice_width = width // tp_count
    half_width = width // 2
    feed_width = w_query.shape[0]
    bf16 = jnp.bfloat16
    floats = functools.partial(jnp.dot, preferred_element_type=jnp.float32)

    fed = [columns_at(hidden_in, group_index, feed_width)]
    for distance in range(1, ep_count):
        fed.append(
            swapped(columns_at(hidden_in, group_index ^ distance, feed_width), "ep", distance)
        )
    hidden_wide = wide(hidden_in)
    row_scale = lax.rsqrt(jnp.mean(hidden_wide * hidden_wide, -1, keepdims=True) + norm_eps)
    normed = (hidden_wide * row_scale * mix_gain).astype(bf16)
    gate_pre = jnp.einsum("sd,gdh->gsh", normed, w_gates, preferred_element_type=jnp.float32)
    gate_pre = gate_pre + gate_bias[:, None, :]
    carried = jax.nn.log_sigmoid(gate_pre[1]) + state_max
    new_max = jnp.maximum(carried, gate_pre[0])
    forget_weight = jnp.exp(carried - new_max)[..., None]
    input_weight = jnp.exp(gate_pre[0] - new_max)[..., None]

    feed_gain = lax.dynamic_slice_in_dim(mix_gain, group_index * feed_width, feed_width, 0)
    fed = jnp.concatenate(fed, 0)
    fed = (wide(fed) * feed_gain).astype(bf16)
    joined = jnp.concatenate([w_query, w_key, w_value, w_outgate], 1)
    partial = floats(fed, joined).astype(bf16)
    projected = wide(partial[:seq_rows])
    for distance in range(1, ep_count):
        block = partial[distance * seq_rows : (distance + 1) * seq_rows]
        projected = projected + wide(swapped(block, "ep", distance))
    projected = (projected * row_scale).astype(bf16)
    head_cols = heads_dev * head_dim

    def heads_of(role_index):
        part = projected[:, role_index * head_cols : (role_index + 1) * head_cols]
        return part.astype(jnp.float32).reshape(seq_rows, heads_dev, head_dim)

    query_heads = heads_of(0)
    key_heads = heads_of(1) * head_dim ** (-0.5)
    value_heads = heads_of(2)
    out_gate = heads_of(3)
    new_norm = forget_weight * state_norm + input_weight * key_heads
    new_matrix = (
        forget_weight[..., None] * state_matrix
        + (input_weight * value_heads)[..., :, None] * key_heads[..., None, :]
    )
    recalled = jnp.einsum(
        "shek,shk->she", state_matrix, query_heads, precision=lax.Precision.HIGHEST
    )
    matched = jnp.sum(key_heads * query_heads, -1, keepdims=True)
    numerator = forget_weight * recalled + input_weight * value_heads * matched
    denominator = jnp.maximum(jnp.abs(jnp.sum(new_norm * query_heads, -1)), 1.0)
    gated_out = (jax.nn.sigmoid(out_gate) * numerator / denominator[..., None]).reshape(
        seq_rows, head_cols
    )
    gated_out = gated_out.astype(bf16)

    def core_halves(array):
        cut = array.reshape(array.shape[0], chip_count, 2, slice_width)
        mine = lax.dynamic_index_in_dim(cut, core_index, 2, False)
        theirs = lax.dynamic_index_in_dim(cut, 1 - core_index, 2, False)
        flat = (array.shape[0], half_width)
        return mine.reshape(flat), theirs.reshape(flat)

    def chip_sum(array):
        mine, theirs = core_halves(array.astype(bf16))
        return wide(mine) + wide(swapped(theirs, "tp", 1))

    def chip_scatter(array):
        total = wide(columns_at(array, chip_index, slice_width))
        for distance in range(1, chip_count):
            block = columns_at(array, chip_index ^ distance, slice_width)
            total = total + wide(swapped(block, "tp", 2 * distance))
        return total

    mixed_half = chip_sum(floats(gated_out, w_mix_out)).astype(bf16)
    mixed_own = chip_scatter(mixed_half)
    residual_own = columns_at(hidden_in, column_index, slice_width)
    stream_own = (wide(residual_own) + mixed_own).astype(bf16)

    own_routes = lax.dynamic_slice_in_dim(routes, group_index * seq_rows, seq_rows, 0)
    places = jnp.arange(ep_count * group_slots, dtype=jnp.int32)
    place_group = (places // group_slots) ^ group_index
    place_expert = place_group * local_experts + places % group_slots // capacity
    named = own_routes[:, :, None] == place_expert[None, None, :]
    named_any = jnp.any(named, 1)
    before = jnp.arange(seq_rows)[:, None] > jnp.arange(seq_rows)[None, :]
    ranks = floats(before.astype(bf16), named_any.astype(bf16))
    chosen = named_any & (ranks == (places % capacity).astype(jnp.float32)[None, :])
    weights = jnp.sum(jnp.where(named, route_weights[:, :, None], 0.0), 1)
    weights = jnp.where(chosen, weights, 0.0)
    chooser = chosen.astype(bf16).T

    pieces = [stream_own]
    for distance in range(1, chip_count):
        pieces.append(swapped(stream_own, "tp", 2 * distance))
    stream_half = jnp.concatenate(
        [pick_chip(pieces, chip_index ^ place) for place in range(chip_count)], 1
    )
    arrived = []
    for distance in range(ep_count):
        block_chooser = chooser[distance * group_slots : (distance + 1) * group_slots]
        block = floats(block_chooser, stream_half).astype(bf16)
        arrived.append(swapped(block, "ep", distance) if distance else block)
    own_half = stream_half
    rows_half = jnp.concatenate(arrived, 0)

    own_other = swapped(own_half, "tp", 1)
    rows_other = swapped(rows_half, "tp", 1)
    mine, theirs = feed_forward(
        core_index.reshape(1).astype(jnp.int32),
        (own_half, own_other, rows_half, rows_other, ffn_gain.reshape(1, width)),
        (expert_gate, expert_up, expert_down, shared_gate, shared_up, shared_down),
        slice_width,
        capacity,
    )
    chip_part = wide(mine) + wide(swapped(theirs, "tp", 1))
    shared_half = chip_part[:seq_rows]
    routed_half = chip_part[seq_rows:].astype(bf16)
    returned = []
    for distance in range(ep_count):
        block = routed_half[distance * group_slots : (distance + 1) * group_slots]
        returned.append(swapped(block, "ep", distance) if distance else block)
    returned = jnp.concatenate(returned, 0)
    routed = jnp.dot(weights, wide(returned), precision=lax.Precision.HIGHEST)
    added_own = chip_scatter((routed + shared_half).astype(bf16))
    result = (wide(stream_own) + added_own).astype(bf16)
    return (result, new_matrix, new_norm, new_max)


def pick_chip(pieces, place):
    chosen = pieces[0]
    for distance in range(1, len(pieces)):
        chosen = jnp.where(place == distance, pieces[distance], chosen)
    return chosen


def solution(mesh):
    placed = (
        P("ep", None),
        P(),
        P("ep", "tp"),
        P("ep", "tp"),
        P("ep", "tp"),
        P("ep", "tp"),
        P(None, None, "tp"),
        P(None, "tp"),
        P("ep", "tp", None, None),
        P("ep", "tp", None),
        P("ep", "tp"),
        P("tp", None),
        P(),
        P(),
        P("ep", None),
        P("ep", None, "tp"),
        P("ep", None, "tp"),
        P("ep", "tp", None),
        P(None, "tp"),
        P(None, "tp"),
        P("tp", None),
    )
    return jax.shard_map(
        per_device,
        mesh=mesh,
        in_specs=placed,
        out_specs=(P("ep", "tp"), P("ep", "tp", None, None), P("ep", "tp", None), P("ep", "tp")),
        check_vma=False,
    )
```

time: 208 us -> 89.1 us (0.43)
  waiting for transfers between devices: 108 us -> 25.1 us
  blocking collectives: 32.4 us -> 0 us
  starting transfers between devices: 8.96 us -> 28.4 us
  matrix products: 24.5 us -> 10.8 us
  between operations: 14 us -> 1.01 us
  Pallas kernels: 0 us -> 8.83 us
  local copies, waits for them, and re-layouts: 9.69 us -> 4.98 us
    reduce_scatter x4 -> x0, waiting for transfers between devices: 98.8 us -> none  [the longest x1 30.2 us: per_device(): lax.psum_scatter(mixed_part.astype(jnp.bfloat16), 'tp', scatter_dimension...]
    ppermute x0 -> x25, starting transfers between devices: none -> 28.4 us  [swapped(): lax.ppermute(block, axis, [(source, source ^ distance) for source in rang...]
    ppermute x0 -> x25, waiting for transfers between devices: none -> 25.1 us  [swapped(): lax.ppermute(block, axis, [(source, source ^ distance) for source in rang...]
    all_to_all x1 -> x0, blocking collectives: 18.2 us -> none  [per_device(): lax.all_to_all(outgoing, 'ep', split_axis=0, concat_axis=1, tiled=True)]
    all_gather x1 -> x0, blocking collectives: 14.2 us -> none  [per_device(): stream = lax.all_gather(stream_own, 'tp', axis=1, tiled=True)]
    dot_general x9, matrix products: 23.5 us -> 9.56 us  [the longest x1 5.54 us: per_device(): jnp.einsum('shek,shk->she', state_matrix, query_heads, precision=lax.Prec...]
    all_to_all x2 -> x0, waiting for transfers between devices: 9.1 us -> none  [the longest x1 4.78 us: per_device(): lax.all_to_all(expert_rows.reshape(local_experts, slot_count, slice_width...]
    all_to_all x2 -> x0, starting transfers between devices: 8.83 us -> none  [the longest x1 5.19 us: per_device(): lax.all_to_all(normed, 'ep', split_axis=1, concat_axis=0, tiled=True)]
  transfers between devices with their start and end apart: 6 -> 25, of which waited for: 6 -> 17; matrix products, arithmetic and copies ran while one was open for 4% -> 9% of each run, Pallas kernels for 0% -> 0%
where the time goes in v1:
time: 89.1 us; the launch traced here: 88.7 us
  starting transfers between devices  28.4 us (32%)
  waiting for transfers between devices  25.1 us (28%)
  matrix products  10.8 us (12%)
  other arithmetic  9.51 us (11%)
  Pallas kernels  8.83 us (10%)
  local copies, waits for them, and re-layouts  4.98 us (6%)
  between operations  1.01 us (1%)
    ppermute x25, starting transfers between devices, swapped(): lax.ppermute(block, axis, [(source, source ^ distance) for source in rang...  28.4 us
    ppermute x25, waiting for transfers between devices, swapped(): lax.ppermute(block, axis, [(source, source ^ distance) for source in rang...  25.1 us
    pallas_call x1, Pallas kernels, feed_forward(): pl.pallas_call(kernel, out_shape=(out, out), in_specs=[pl.BlockSpec(memor...  8.83 us
    dot_general x1, matrix products, per_device(): jnp.einsum('shek,shk->she', state_matrix, query_heads, precision=lax.Prec...  5.54 us
    add x1, other arithmetic, per_device(): forget_weight[..., None] * state_matrix  3.29 us
    dot_general x1, matrix products, per_device(): partial = floats(fed, joined).astype(bf16)  1.99 us
  transfers between devices with their start and end apart: 25, of which 17 were waited for; matrix products, arithmetic and copies ran while one was open for 9% of the time, Pallas kernels for 0%

profile of v1, /device:TPU:0, one launch (start us, length us, event | category | flops | bytes accessed | tf_op | source)
XLA Modules:
  0.0 88.7 jit_solution(14262654514233867243)
XLA Ops:
  0.7 1.1 %constant_dynamic-slice_fusion.10 = (bf16[32,1024]{1,0:T(8,128)(2,1)S(1)}, bf16[32,1024]{1,0:T(8,128)(2,1)S(1)}, bf16[32,1024]{1,0:T(8,128)(2,1)S(1)}, bf16[32,1024]{1,0:T(8,128)(2,1)S(1)}) fusion(bf16[32,4096]{1,0:T(8,128)(2,1)} %param.21, s32[]{:T(128)S(6)} %select_n.175, s32[]{:T(128)S(6)} %select_n.177, s32[]{:T(128)S(6)} %select_n.176, s32[]{:T(128)S(6)} %select_n.178), kind=kLoop, calls=%fused_computation.96 | loop fusion | bytes 524304 | tf_op jit(solution)/shard_map/dynamic_slice | solution.py:24
  1.8 3.1 %collective-permute-start.1 = (bf16[32,1024]{1,0:T(8,128)(2,1)S(1)}, bf16[32,1024]{1,0:T(8,128)(2,1)S(1)}, u32[]{:S(2)}, u32[]{:S(2)}) collective-permute-start(bf16[32,1024]{1,0:T(8,128)(2,1)S(1)} %get-tuple-element.26), channel_id=1, source_target_pairs={{0,16},{8,24},{16,0},{24,8},{1,17},{9,25},{17,1},{25,9},{2,18},{10... | collective-permute-start | bytes 196616 | tf_op jit(solution)/shard_map/ppermute | solution.py:20
  4.8 1.5 %collective-permute-start = (bf16[32,1024]{1,0:T(8,128)(2,1)S(1)}, bf16[32,1024]{1,0:T(8,128)(2,1)S(1)}, u32[]{:S(2)}, u32[]{:S(2)}) collective-permute-start(bf16[32,1024]{1,0:T(8,128)(2,1)S(1)} %get-tuple-element.27), channel_id=1, source_target_pairs={{0,8},{8,0},{16,24},{24,16},{1,9},{9,1},{17,25},{25,17},{2,10},{10... | collective-permute-start | bytes 196616 | tf_op jit(solution)/shard_map/ppermute | solution.py:20
  6.4 1.1 %fusion.20 = f32[32]{0:T(128)S(1)} fusion(bf16[32,4096]{1,0:T(8,128)(2,1)} %param.21), kind=kLoop, calls=%fused_computation.30 | loop fusion | flops 393184 | bytes 262272 | tf_op jit(solution)/shard_map/reduce_sum | solution.py:197
  7.5 0.7 dynamic_slice.57
  8.2 1.2 %fusion.19 = f32[2,32,4]{1,2,0:T(4,128)S(1)} fusion(bf16[2,4096,4]{1,2,0:T(4,128)(2,1)} %param.27, bf16[32,4096]{1,0:T(8,128)(2,1)} %param.21, f32[4096]{0:T(1024)} %param.22, f32[32]{0:T(128)S(1)} %add_rsqrt_fusion, f32[2,4]{1,0:T(2,128)} %param.28), kind=kOutput, calls=%fused_computation.26 | convolution fusion | flops 2621696 | bytes 345248 | tf_op jit(solution)/shard_map/sd,gdh->gsh/dot_general | solution.py:199
  9.4 0.7 subtract_exponential_fusion.1
  10.5 1.0 %collective-permute-done.2 = bf16[32,1024]{1,0:T(8,128)(2,1)S(1)} collective-permute-done((bf16[32,1024]{1,0:T(8,128)(2,1)S(1)}, bf16[32,1024]{1,0:T(8,128)(2,1)S(1)}, u32[]{:S(2)}, u32[]{:S(2)}) %collective-permute-start.2) | collective-permute-done | bytes 65568 | tf_op jit(solution)/shard_map/ppermute | solution.py:20
  11.5 2.0 %fusion.10 = bf16[128,1024]{1,0:T(8,128)(2,1)S(1)} fusion(bf16[1024,256]{1,0:T(8,128)(2,1)} %param.26, bf16[1024,256]{1,0:T(8,128)(2,1)} %param.25, bf16[1024,256]{1,0:T(8,128)(2,1)} %param.24, bf16[1024,256]{1,0:T(8,128)(2,1)} %param.23, bf16[32,1024]{1,0:T(8,128)(2,1)S(1)} %collective-permute-done.2, bf16[32,1024]{1,0:T(8,128)(2,1)S(1)} %collective-permute-done.1, ...), kind=kOutput, calls=%fused_computation.17 | convolution fusion | flops 278265856 | bytes 2625536 | tf_op jit(solution)/shard_map/dot_general | solution.py:210
  13.5 1.0 %collective-permute-start.3 = (bf16[32,1024]{1,0:T(8,128)(2,1)S(1)}, bf16[32,1024]{1,0:T(8,128)(2,1)S(1)}, u32[]{:S(2)}, u32[]{:S(2)}) collective-permute-start(bf16[32,1024]{1,0:T(8,128)(2,1)S(1)} %get-tuple-element.22), channel_id=1, source_target_pairs={{0,8},{8,0},{16,24},{24,16},{1,9},{9,1},{17,25},{25,17},{2,10},{10... | collective-permute-start | bytes 196616 | tf_op jit(solution)/shard_map/ppermute | solution.py:20
  14.5 1.5 %collective-permute-start.5 = (bf16[32,1024]{1,0:T(8,128)(2,1)S(1)}, bf16[32,1024]{1,0:T(8,128)(2,1)S(1)}, u32[]{:S(2)}, u32[]{:S(2)}) collective-permute-start(bf16[32,1024]{1,0:T(8,128)(2,1)S(1)} %get-tuple-element.23), channel_id=1, source_target_pairs={{0,24},{8,16},{16,8},{24,0},{1,25},{9,17},{17,9},{25,1},{2,26},{10... | collective-permute-start | bytes 196616 | tf_op jit(solution)/shard_map/ppermute | solution.py:20
  16.0 1.1 %collective-permute-start.4 = (bf16[32,1024]{1,0:T(8,128)(2,1)S(1)}, bf16[32,1024]{1,0:T(8,128)(2,1)S(1)}, u32[]{:S(2)}, u32[]{:S(2)}) collective-permute-start(bf16[32,1024]{1,0:T(8,128)(2,1)S(1)} %get-tuple-element.24), channel_id=1, source_target_pairs={{0,16},{8,24},{16,0},{24,8},{1,17},{9,25},{17,1},{25,9},{2,18},{10... | collective-permute-start | bytes 196616 | tf_op jit(solution)/shard_map/ppermute | solution.py:20
  17.2 1.0 %collective-permute-done.3 = bf16[32,1024]{1,0:T(8,128)(2,1)S(1)} collective-permute-done((bf16[32,1024]{1,0:T(8,128)(2,1)S(1)}, bf16[32,1024]{1,0:T(8,128)(2,1)S(1)}, u32[]{:S(2)}, u32[]{:S(2)}) %collective-permute-start.3) | collective-permute-done | bytes 65568 | tf_op jit(solution)/shard_map/ppermute | solution.py:20
  18.2 1.5 %collective-permute-done.5 = bf16[32,1024]{1,0:T(8,128)(2,1)S(1)} collective-permute-done((bf16[32,1024]{1,0:T(8,128)(2,1)S(1)}, bf16[32,1024]{1,0:T(8,128)(2,1)S(1)}, u32[]{:S(2)}, u32[]{:S(2)}) %collective-permute-start.5) | collective-permute-done | bytes 65568 | tf_op jit(solution)/shard_map/ppermute | solution.py:20
  19.7 0.7 collective-permute-done.4
  21.0 0.8 fusion.42
  21.8 5.5 %fusion.66 = f32[32,4,1,64]{3,2,1,0:T(1,128)S(1)} fusion(bf16[32,4,64,1]{2,3,1,0:T(2,128)(2,1)S(1)} %reshape.141, f32[32,4,64,64]{3,2,1,0:T(8,128)} %param.29), kind=kOutput, calls=%fused_computation.125 | convolution fusion | flops 6291456 | bytes 2146304 | tf_op jit(solution)/shard_map/shek,shk->she/dot_general | solution.py:231
  27.3 0.5 fusion.17
  27.9 0.1 convert_element_type.139
  28.0 0.5 convolution_convert_fusion
  28.4 0.2 reshape.128
  28.6 1.1 %dynamic-slice_reduce_fusion = (bf16[32,4,512]{2,1,0:T(4,128)(2,1)S(1)}, bf16[32,4,1,512]{3,2,1,0:T(2,128)(2,1)S(1)}) fusion(bf16[32,4,2,512]{3,2,1,0:T(2,128)(2,1)S(1)} %reshape.128, s32[]{:T(128)S(6)} %select_n.182, s32[]{:T(128)S(6)} %select_n.181), kind=kLoop, calls=%fused_computation.51 | loop fusion | bytes 524296 | tf_op jit(solution)/shard_map/jit(dynamic_index_in_dim)/dynamic_slice | solution.py:245
  30.0 1.2 %collective-permute-done.6 = bf16[32,2048]{1,0:T(8,128)(2,1)S(1)} collective-permute-done((bf16[32,2048]{1,0:T(8,128)(2,1)S(1)}, bf16[32,2048]{1,0:T(8,128)(2,1)S(1)}, u32[]{:S(2)}, u32[]{:S(2)}) %collective-permute-start.6) | collective-permute-done | bytes 131104 | tf_op jit(solution)/shard_map/ppermute | solution.py:20
  31.2 1.6 %collective-permute-start.7 = (bf16[32,512]{1,0:T(8,128)(2,1)S(1)}, bf16[32,512]{1,0:T(8,128)(2,1)S(1)}, u32[]{:S(2)}, u32[]{:S(2)}) collective-permute-start(bf16[32,512]{1,0:T(8,128)(2,1)S(1)} %get-tuple-element.36), channel_id=1, source_target_pairs={{0,2},{1,3},{2,0},{3,1},{4,6},{5,7},{6,4},{7,5},{8,10},{9,11},{10,... | collective-permute-start | bytes 98312 | tf_op jit(solution)/shard_map/ppermute | solution.py:20
  32.9 2.5 %collective-permute-start.9 = (bf16[32,512]{1,0:T(8,128)(2,1)S(1)}, bf16[32,512]{1,0:T(8,128)(2,1)S(1)}, u32[]{:S(2)}, u32[]{:S(2)}) collective-permute-start(bf16[32,512]{1,0:T(8,128)(2,1)S(1)} %get-tuple-element.37), channel_id=1, source_target_pairs={{0,6},{1,7},{2,4},{3,5},{4,2},{5,3},{6,0},{7,1},{8,14},{9,15},{10,... | collective-permute-start | bytes 98312 | tf_op jit(solution)/shard_map/ppermute | solution.py:20
  35.4 0.1 collective-permute-start.8
  35.6 3.1 %collective-permute-done.9 = bf16[32,512]{1,0:T(8,128)(2,1)S(1)} collective-permute-done((bf16[32,512]{1,0:T(8,128)(2,1)S(1)}, bf16[32,512]{1,0:T(8,128)(2,1)S(1)}, u32[]{:S(2)}, u32[]{:S(2)}) %collective-permute-start.9) | collective-permute-done | bytes 32800 | tf_op jit(solution)/shard_map/ppermute | solution.py:20
  38.6 1.9 %collective-permute-done.8 = bf16[32,512]{1,0:T(8,128)(2,1)S(1)} collective-permute-done((bf16[32,512]{1,0:T(8,128)(2,1)S(1)}, bf16[32,512]{1,0:T(8,128)(2,1)S(1)}, u32[]{:S(2)}, u32[]{:S(2)}) %collective-permute-start.8) | collective-permute-done | bytes 32800 | tf_op jit(solution)/shard_map/ppermute | solution.py:20
  40.5 0.8 add_convert_fusion.2
  41.3 0.5 collective-permute-start.12
  41.8 1.7 %collective-permute-start.11 = (bf16[32,512]{1,0:T(8,128)(2,1)S(1)}, bf16[32,512]{1,0:T(8,128)(2,1)S(1)}, u32[]{:S(2)}, u32[]{:S(2)}) collective-permute-start(bf16[32,512]{1,0:T(8,128)(2,1)S(1)} %add_convert_fusion.2), channel_id=1, source_target_pairs={{0,4},{1,5},{2,6},{3,7},{4,0},{5,1},{6,2},{7,3},{8,12},{9,13},{10,... | collective-permute-start | bytes 98312 | tf_op jit(solution)/shard_map/ppermute | solution.py:20
  43.5 2.3 %collective-permute-start.10 = (bf16[32,512]{1,0:T(8,128)(2,1)S(1)}, bf16[32,512]{1,0:T(8,128)(2,1)S(1)}, u32[]{:S(2)}, u32[]{:S(2)}) collective-permute-start(bf16[32,512]{1,0:T(8,128)(2,1)S(1)} %add_convert_fusion.2), channel_id=1, source_target_pairs={{0,6},{1,7},{2,4},{3,5},{4,2},{5,3},{6,0},{7,1},{8,14},{9,15},{10,... | collective-permute-start | bytes 98312 | tf_op jit(solution)/shard_map/ppermute | solution.py:20
  45.8 0.1 fusion.18
  45.9 0.7 collective-permute-done.11
  46.6 2.6 %collective-permute-done.10 = bf16[32,512]{1,0:T(8,128)(2,1)S(1)} collective-permute-done((bf16[32,512]{1,0:T(8,128)(2,1)S(1)}, bf16[32,512]{1,0:T(8,128)(2,1)S(1)}, u32[]{:S(2)}, u32[]{:S(2)}) %collective-permute-start.10) | collective-permute-done | bytes 32800 | tf_op jit(solution)/shard_map/ppermute | solution.py:20
  49.2 0.3 convolution_convert_fusion.3
  49.5 0.3 convolution_convert_fusion.2
  49.8 0.3 convolution_convert_fusion.1
  50.1 1.6 %collective-permute-start.16 = (bf16[18,2048]{1,0:T(8,128)(2,1)S(1)}, bf16[18,2048]{1,0:T(8,128)(2,1)S(1)}, u32[]{:S(2)}, u32[]{:S(2)}) collective-permute-start(bf16[18,2048]{1,0:T(8,128)(2,1)S(1)} %convolution_convert_fusion.1), channel_id=1, source_target_pairs={{0,24},{8,16},{16,8},{24,0},{1,25},{9,17},{17,9},{25,1},{2,26},{10... | collective-permute-start | bytes 221192 | tf_op jit(solution)/shard_map/ppermute | solution.py:20
  51.7 1.4 %collective-permute-start.15 = (bf16[18,2048]{1,0:T(8,128)(2,1)S(1)}, bf16[18,2048]{1,0:T(8,128)(2,1)S(1)}, u32[]{:S(2)}, u32[]{:S(2)}) collective-permute-start(bf16[18,2048]{1,0:T(8,128)(2,1)S(1)} %convolution_convert_fusion.2), channel_id=1, source_target_pairs={{0,16},{8,24},{16,0},{24,8},{1,17},{9,25},{17,1},{25,9},{2,18},{10... | collective-permute-start | bytes 221192 | tf_op jit(solution)/shard_map/ppermute | solution.py:20
  53.0 0.6 collective-permute-start.14
  53.7 0.2 convolution_convert_fusion.4
  53.9 1.9 %collective-permute-done.16 = bf16[18,2048]{1,0:T(8,128)(2,1)S(1)} collective-permute-done((bf16[18,2048]{1,0:T(8,128)(2,1)S(1)}, bf16[18,2048]{1,0:T(8,128)(2,1)S(1)}, u32[]{:S(2)}, u32[]{:S(2)}) %collective-permute-start.16) | collective-permute-done | bytes 73760 | tf_op jit(solution)/shard_map/ppermute | solution.py:20
  55.7 1.0 %collective-permute-done.15 = bf16[18,2048]{1,0:T(8,128)(2,1)S(1)} collective-permute-done((bf16[18,2048]{1,0:T(8,128)(2,1)S(1)}, bf16[18,2048]{1,0:T(8,128)(2,1)S(1)}, u32[]{:S(2)}, u32[]{:S(2)}) %collective-permute-start.15) | collective-permute-done | bytes 73760 | tf_op jit(solution)/shard_map/ppermute | solution.py:20
  56.7 0.9 %collective-permute-done.14 = bf16[18,2048]{1,0:T(8,128)(2,1)S(1)} collective-permute-done((bf16[18,2048]{1,0:T(8,128)(2,1)S(1)}, bf16[18,2048]{1,0:T(8,128)(2,1)S(1)}, u32[]{:S(2)}, u32[]{:S(2)}) %collective-permute-start.14) | collective-permute-done | bytes 73760 | tf_op jit(solution)/shard_map/ppermute | solution.py:20
  57.9 0.6 collective-permute-start.13
  58.4 1.2 %collective-permute-done.13.own_other = bf16[32,2048]{1,0:T(8,128)(2,1)S(1)} collective-permute-done((bf16[32,2048]{1,0:T(8,128)(2,1)S(1)}, bf16[32,2048]{1,0:T(8,128)(2,1)S(1)}, u32[]{:S(2)}, u32[]{:S(2)}) %collective-permute-start.13) | collective-permute-done | bytes 131104 | tf_op jit(solution)/shard_map/ppermute | solution.py:20
  59.6 0.6 copy-done.5
  60.2 0.1 copy-done.4
  60.4 8.8 %feed_forward.1 = (bf16[104,2048]{1,0:T(8,128)(2,1)}, bf16[104,2048]{1,0:T(8,128)(2,1)}) custom-call(s32[1]{0:T(128)} %bitcast.7.core, bf16[32,2048]{1,0:T(8,128)(2,1)} %copy-done.3, bf16[32,2048]{1,0:T(8,128)(2,1)} %copy-done.5, bf16[72,2048]{1,0:T(8,128)(2,1)} %copy-done.2, bf16[72,2048]{1,0:T(8,128)(2,1)} %copy-done.4, f32[1,4096]{1,0:T(1,128)} %bitcast.45, ...), custom_call_target="tpu_custom_call" | custom-call | tf_op jit(solution)/shard_map/feed_forward/pallas_call | solution.py:136
  69.2 0.2 collective-permute-start.18
  69.4 1.8 %collective-permute-done.18 = bf16[104,2048]{1,0:T(8,128)(2,1)S(1)} collective-permute-done((bf16[104,2048]{1,0:T(8,128)(2,1)}, bf16[104,2048]{1,0:T(8,128)(2,1)S(1)}, u32[]{:S(2)}, u32[]{:S(2)}) %collective-permute-start.18) | collective-permute-done | bytes 426016 | tf_op jit(solution)/shard_map/ppermute | solution.py:20
  71.2 1.1 %convert_add_fusion = (f32[104,2048]{1,0:T(8,128)S(1)}, bf16[104,2048]{1,0:T(8,128)(2,1)S(1)}) fusion(bf16[104,2048]{1,0:T(8,128)(2,1)S(1)} %collective-permute-done.18, bf16[104,2048]{1,0:T(8,128)(2,1)} %get-tuple-element.6), kind=kLoop, calls=%fused_computation.27 | loop fusion | flops 851968 | bytes 2129920 | tf_op jit(solution)/shard_map/add | solution.py:301
  72.5 1.7 %collective-permute-start.21 = (bf16[18,2048]{1,0:T(8,128)(2,1)S(1)}, bf16[18,2048]{1,0:T(8,128)(2,1)S(1)}, u32[]{:S(2)}, u32[]{:S(2)}) collective-permute-start(bf16[18,2048]{1,0:T(8,128)(2,1)S(1)} %get-tuple-element.17), channel_id=1, source_target_pairs={{0,24},{8,16},{16,8},{24,0},{1,25},{9,17},{17,9},{25,1},{2,26},{10... | collective-permute-start | bytes 221192 | tf_op jit(solution)/shard_map/ppermute | solution.py:20
  74.1 0.5 collective-permute-start.20
  74.6 1.4 %collective-permute-start.19 = (bf16[18,2048]{1,0:T(8,128)(2,1)S(1)}, bf16[18,2048]{1,0:T(8,128)(2,1)S(1)}, u32[]{:S(2)}, u32[]{:S(2)}) collective-permute-start(bf16[18,2048]{1,0:T(8,128)(2,1)S(1)} %get-tuple-element.19), channel_id=1, source_target_pairs={{0,8},{8,0},{16,24},{24,16},{1,9},{9,1},{17,25},{25,17},{2,10},{10... | collective-permute-start | bytes 221192 | tf_op jit(solution)/shard_map/ppermute | solution.py:20
  76.1 2.7 %collective-permute-done.21 = bf16[18,2048]{1,0:T(8,128)(2,1)S(1)} collective-permute-done((bf16[18,2048]{1,0:T(8,128)(2,1)S(1)}, bf16[18,2048]{1,0:T(8,128)(2,1)S(1)}, u32[]{:S(2)}, u32[]{:S(2)}) %collective-permute-start.21) | collective-permute-done | bytes 73760 | tf_op jit(solution)/shard_map/ppermute | solution.py:20
  78.8 1.6 %collective-permute-done.20 = bf16[18,2048]{1,0:T(8,128)(2,1)S(1)} collective-permute-done((bf16[18,2048]{1,0:T(8,128)(2,1)S(1)}, bf16[18,2048]{1,0:T(8,128)(2,1)S(1)}, u32[]{:S(2)}, u32[]{:S(2)}) %collective-permute-start.20) | collective-permute-done | bytes 73760 | tf_op jit(solution)/shard_map/ppermute | solution.py:20
  80.4 0.3 fusion.1
  80.9 2.3 %collective-permute-start.24 = (bf16[32,512]{1,0:T(8,128)(2,1)S(1)}, bf16[32,512]{1,0:T(8,128)(2,1)S(1)}, u32[]{:S(2)}, u32[]{:S(2)}) collective-permute-start(bf16[32,512]{1,0:T(8,128)(2,1)S(1)} %get-tuple-element.30), channel_id=1, source_target_pairs={{0,6},{1,7},{2,4},{3,5},{4,2},{5,3},{6,0},{7,1},{8,14},{9,15},{10,... | collective-permute-start | bytes 98312 | tf_op jit(solution)/shard_map/ppermute | solution.py:20
  83.2 1.1 %collective-permute-start.23 = (bf16[32,512]{1,0:T(8,128)(2,1)S(1)}, bf16[32,512]{1,0:T(8,128)(2,1)S(1)}, u32[]{:S(2)}, u32[]{:S(2)}) collective-permute-start(bf16[32,512]{1,0:T(8,128)(2,1)S(1)} %get-tuple-element.31), channel_id=1, source_target_pairs={{0,4},{1,5},{2,6},{3,7},{4,0},{5,1},{6,2},{7,3},{8,12},{9,13},{10,... | collective-permute-start | bytes 98312 | tf_op jit(solution)/shard_map/ppermute | solution.py:20
  84.3 3.3 %multiply_add_fusion = f32[32,4,64,64]{3,2,1,0:T(8,128)} fusion(f32[32,4,64,64]{3,2,1,0:T(8,128)S(1)} %copy-done.1, f32[32,4,64]{2,1,0:T(4,128)S(1)} %get-tuple-element.39, f32[32,4,64]{2,1,0:T(4,128)S(1)} %get-tuple-element.45, f32[32,4]{1,0:T(8,128)S(1)} %copy.33), kind=kLoop, calls=%fused_computation.2 | loop fusion | flops 1572864 | bytes 4260352 | tf_op jit(solution)/shard_map/add | solution.py:228
  87.6 0.4 collective-permute-done.23
  88.0 0.6 add_convert_fusion.1
  (59 shorter events, 1.9 us)
Async XLA Ops:
  0.6 27.3 %copy-start = (bf16[256,4096]{1,0:T(8,128)(2,1)S(1)}, bf16[256,4096]{1,0:T(8,128)(2,1)}, u32[]{:S(2)}) copy-start(bf16[256,4096]{1,0:T(8,128)(2,1)} %param.32) | copy-start | bytes 6291460
  1.8 8.7 %collective-permute-start.1 = (bf16[32,1024]{1,0:T(8,128)(2,1)S(1)}, bf16[32,1024]{1,0:T(8,128)(2,1)S(1)}, u32[]{:S(2)}, u32[]{:S(2)}) collective-permute-start(bf16[32,1024]{1,0:T(8,128)(2,1)S(1)} %get-tuple-element.26), channel_id=1, source_target_pairs={{0,16},{8,24},{16,0},{24,8},{1,17},{9,25},{17,1},{25,9},{2,18},{10... | collective-permute-start | bytes 196616 | tf_op jit(solution)/shard_map/ppermute | solution.py:20
  4.8 5.6 %collective-permute-start = (bf16[32,1024]{1,0:T(8,128)(2,1)S(1)}, bf16[32,1024]{1,0:T(8,128)(2,1)S(1)}, u32[]{:S(2)}, u32[]{:S(2)}) collective-permute-start(bf16[32,1024]{1,0:T(8,128)(2,1)S(1)} %get-tuple-element.27), channel_id=1, source_target_pairs={{0,8},{8,0},{16,24},{24,16},{1,9},{9,1},{17,25},{25,17},{2,10},{10... | collective-permute-start | bytes 196616 | tf_op jit(solution)/shard_map/ppermute | solution.py:20
  6.3 5.2 %collective-permute-start.2 = (bf16[32,1024]{1,0:T(8,128)(2,1)S(1)}, bf16[32,1024]{1,0:T(8,128)(2,1)S(1)}, u32[]{:S(2)}, u32[]{:S(2)}) collective-permute-start(bf16[32,1024]{1,0:T(8,128)(2,1)S(1)} %get-tuple-element.28), channel_id=1, source_target_pairs={{0,24},{8,16},{16,8},{24,0},{1,25},{9,17},{17,9},{25,1},{2,26},{10... | collective-permute-start | bytes 196616 | tf_op jit(solution)/shard_map/ppermute | solution.py:20
  10.1 3.4 %copy-start.7 = (f32[32,4]{0,1:T(4,128)}, f32[32,4]{0,1:T(4,128)S(1)}, u32[]{:S(2)}) copy-start(f32[32,4]{0,1:T(4,128)S(1)} %get-tuple-element.11) | copy-start | bytes 1540
  11.5 5.6 %copy-start.9 = (s32[128,2]{0,1:T(2,128)S(1)}, s32[128,2]{0,1:T(2,128)}, u32[]{:S(2)}) copy-start(s32[128,2]{0,1:T(2,128)} %param.34) | copy-start | bytes 3076
  11.5 9.5 %copy-start.6 = (f32[32,4,64]{2,1,0:T(4,128)S(1)}, f32[32,4,64]{2,1,0:T(4,128)}, u32[]{:S(2)}) copy-start(f32[32,4,64]{2,1,0:T(4,128)} %param.30) | copy-start | bytes 98308
  13.5 4.7 %collective-permute-start.3 = (bf16[32,1024]{1,0:T(8,128)(2,1)S(1)}, bf16[32,1024]{1,0:T(8,128)(2,1)S(1)}, u32[]{:S(2)}, u32[]{:S(2)}) collective-permute-start(bf16[32,1024]{1,0:T(8,128)(2,1)S(1)} %get-tuple-element.22), channel_id=1, source_target_pairs={{0,8},{8,0},{16,24},{24,16},{1,9},{9,1},{17,25},{25,17},{2,10},{10... | collective-permute-start | bytes 196616 | tf_op jit(solution)/shard_map/ppermute | solution.py:20
  14.5 5.2 %collective-permute-start.5 = (bf16[32,1024]{1,0:T(8,128)(2,1)S(1)}, bf16[32,1024]{1,0:T(8,128)(2,1)S(1)}, u32[]{:S(2)}, u32[]{:S(2)}) collective-permute-start(bf16[32,1024]{1,0:T(8,128)(2,1)S(1)} %get-tuple-element.23), channel_id=1, source_target_pairs={{0,24},{8,16},{16,8},{24,0},{1,25},{9,17},{17,9},{25,1},{2,26},{10... | collective-permute-start | bytes 196616 | tf_op jit(solution)/shard_map/ppermute | solution.py:20
  16.0 4.4 %collective-permute-start.4 = (bf16[32,1024]{1,0:T(8,128)(2,1)S(1)}, bf16[32,1024]{1,0:T(8,128)(2,1)S(1)}, u32[]{:S(2)}, u32[]{:S(2)}) collective-permute-start(bf16[32,1024]{1,0:T(8,128)(2,1)S(1)} %get-tuple-element.24), channel_id=1, source_target_pairs={{0,16},{8,24},{16,0},{24,8},{1,17},{9,25},{17,1},{25,9},{2,18},{10... | collective-permute-start | bytes 196616 | tf_op jit(solution)/shard_map/ppermute | solution.py:20
  29.8 1.4 %collective-permute-start.6 = (bf16[32,2048]{1,0:T(8,128)(2,1)S(1)}, bf16[32,2048]{1,0:T(8,128)(2,1)S(1)}, u32[]{:S(2)}, u32[]{:S(2)}) collective-permute-start(bf16[32,2048]{1,0:T(8,128)(2,1)S(1)} %bitcast.43), channel_id=1, source_target_pairs={{0,1},{1,0},{2,3},{3,2},{4,5},{5,4},{6,7},{7,6},{8,9},{9,8},{10,11... | collective-permute-start | bytes 393224 | tf_op jit(solution)/shard_map/ppermute | solution.py:20
  31.2 4.3 %collective-permute-start.7 = (bf16[32,512]{1,0:T(8,128)(2,1)S(1)}, bf16[32,512]{1,0:T(8,128)(2,1)S(1)}, u32[]{:S(2)}, u32[]{:S(2)}) collective-permute-start(bf16[32,512]{1,0:T(8,128)(2,1)S(1)} %get-tuple-element.36), channel_id=1, source_target_pairs={{0,2},{1,3},{2,0},{3,1},{4,6},{5,7},{6,4},{7,5},{8,10},{9,11},{10,... | collective-permute-start | bytes 98312 | tf_op jit(solution)/shard_map/ppermute | solution.py:20
  32.9 5.8 %collective-permute-start.9 = (bf16[32,512]{1,0:T(8,128)(2,1)S(1)}, bf16[32,512]{1,0:T(8,128)(2,1)S(1)}, u32[]{:S(2)}, u32[]{:S(2)}) collective-permute-start(bf16[32,512]{1,0:T(8,128)(2,1)S(1)} %get-tuple-element.37), channel_id=1, source_target_pairs={{0,6},{1,7},{2,4},{3,5},{4,2},{5,3},{6,0},{7,1},{8,14},{9,15},{10,... | collective-permute-start | bytes 98312 | tf_op jit(solution)/shard_map/ppermute | solution.py:20
  35.4 5.2 %collective-permute-start.8 = (bf16[32,512]{1,0:T(8,128)(2,1)S(1)}, bf16[32,512]{1,0:T(8,128)(2,1)S(1)}, u32[]{:S(2)}, u32[]{:S(2)}) collective-permute-start(bf16[32,512]{1,0:T(8,128)(2,1)S(1)} %get-tuple-element.38), channel_id=1, source_target_pairs={{0,4},{1,5},{2,6},{3,7},{4,0},{5,1},{6,2},{7,3},{8,12},{9,13},{10,... | collective-permute-start | bytes 98312 | tf_op jit(solution)/shard_map/ppermute | solution.py:20
  41.3 4.6 %collective-permute-start.12 = (bf16[32,512]{1,0:T(8,128)(2,1)S(1)}, bf16[32,512]{1,0:T(8,128)(2,1)S(1)}, u32[]{:S(2)}, u32[]{:S(2)}) collective-permute-start(bf16[32,512]{1,0:T(8,128)(2,1)S(1)} %add_convert_fusion.2), channel_id=1, source_target_pairs={{0,2},{1,3},{2,0},{3,1},{4,6},{5,7},{6,4},{7,5},{8,10},{9,11},{10,... | collective-permute-start | bytes 98312 | tf_op jit(solution)/shard_map/ppermute | solution.py:20
  41.8 4.8 %collective-permute-start.11 = (bf16[32,512]{1,0:T(8,128)(2,1)S(1)}, bf16[32,512]{1,0:T(8,128)(2,1)S(1)}, u32[]{:S(2)}, u32[]{:S(2)}) collective-permute-start(bf16[32,512]{1,0:T(8,128)(2,1)S(1)} %add_convert_fusion.2), channel_id=1, source_target_pairs={{0,4},{1,5},{2,6},{3,7},{4,0},{5,1},{6,2},{7,3},{8,12},{9,13},{10,... | collective-permute-start | bytes 98312 | tf_op jit(solution)/shard_map/ppermute | solution.py:20
  43.5 5.7 %collective-permute-start.10 = (bf16[32,512]{1,0:T(8,128)(2,1)S(1)}, bf16[32,512]{1,0:T(8,128)(2,1)S(1)}, u32[]{:S(2)}, u32[]{:S(2)}) collective-permute-start(bf16[32,512]{1,0:T(8,128)(2,1)S(1)} %add_convert_fusion.2), channel_id=1, source_target_pairs={{0,6},{1,7},{2,4},{3,5},{4,2},{5,3},{6,0},{7,1},{8,14},{9,15},{10,... | collective-permute-start | bytes 98312 | tf_op jit(solution)/shard_map/ppermute | solution.py:20
  50.1 5.6 %collective-permute-start.16 = (bf16[18,2048]{1,0:T(8,128)(2,1)S(1)}, bf16[18,2048]{1,0:T(8,128)(2,1)S(1)}, u32[]{:S(2)}, u32[]{:S(2)}) collective-permute-start(bf16[18,2048]{1,0:T(8,128)(2,1)S(1)} %convolution_convert_fusion.1), channel_id=1, source_target_pairs={{0,24},{8,16},{16,8},{24,0},{1,25},{9,17},{17,9},{25,1},{2,26},{10... | collective-permute-start | bytes 221192 | tf_op jit(solution)/shard_map/ppermute | solution.py:20
  51.7 5.1 %collective-permute-start.15 = (bf16[18,2048]{1,0:T(8,128)(2,1)S(1)}, bf16[18,2048]{1,0:T(8,128)(2,1)S(1)}, u32[]{:S(2)}, u32[]{:S(2)}) collective-permute-start(bf16[18,2048]{1,0:T(8,128)(2,1)S(1)} %convolution_convert_fusion.2), channel_id=1, source_target_pairs={{0,16},{8,24},{16,0},{24,8},{1,17},{9,25},{17,1},{25,9},{2,18},{10... | collective-permute-start | bytes 221192 | tf_op jit(solution)/shard_map/ppermute | solution.py:20
  53.0 4.6 %collective-permute-start.14 = (bf16[18,2048]{1,0:T(8,128)(2,1)S(1)}, bf16[18,2048]{1,0:T(8,128)(2,1)S(1)}, u32[]{:S(2)}, u32[]{:S(2)}) collective-permute-start(bf16[18,2048]{1,0:T(8,128)(2,1)S(1)} %convolution_convert_fusion.3), channel_id=1, source_target_pairs={{0,8},{8,0},{16,24},{24,16},{1,9},{9,1},{17,25},{25,17},{2,10},{10... | collective-permute-start | bytes 221192 | tf_op jit(solution)/shard_map/ppermute | solution.py:20
  57.7 1.9 %copy-start.2 = (bf16[72,2048]{1,0:T(8,128)(2,1)}, bf16[72,2048]{1,0:T(8,128)(2,1)S(1)}, u32[]{:S(2)}) copy-start(bf16[72,2048]{1,0:T(8,128)(2,1)S(1)} %pad_maximum_fusion.routed) | copy-start | bytes 884740
  57.8 1.8 %collective-permute-start.17 = (bf16[72,2048]{1,0:T(8,128)(2,1)S(1)}, bf16[72,2048]{1,0:T(8,128)(2,1)S(1)}, u32[]{:S(2)}, u32[]{:S(2)}) collective-permute-start(bf16[72,2048]{1,0:T(8,128)(2,1)S(1)} %pad_maximum_fusion.routed), channel_id=1, source_target_pairs={{0,1},{1,0},{2,3},{3,2},{4,5},{5,4},{6,7},{7,6},{8,9},{9,8},{10,11... | collective-permute-start | bytes 884744 | tf_op jit(solution)/shard_map/ppermute | solution.py:20
  57.8 1.8 %copy-start.3 = (bf16[32,2048]{1,0:T(8,128)(2,1)}, bf16[32,2048]{1,0:T(8,128)(2,1)S(1)}, u32[]{:S(2)}) copy-start(bf16[32,2048]{1,0:T(8,128)(2,1)S(1)} %pad_maximum_fusion.1.own) | copy-start | bytes 393220
  57.9 1.7 %collective-permute-start.13 = (bf16[32,2048]{1,0:T(8,128)(2,1)S(1)}, bf16[32,2048]{1,0:T(8,128)(2,1)S(1)}, u32[]{:S(2)}, u32[]{:S(2)}) collective-permute-start(bf16[32,2048]{1,0:T(8,128)(2,1)S(1)} %pad_maximum_fusion.1.own), channel_id=1, source_target_pairs={{0,1},{1,0},{2,3},{3,2},{4,5},{5,4},{6,7},{7,6},{8,9},{9,8},{10,11... | collective-permute-start | bytes 393224 | tf_op jit(solution)/shard_map/ppermute | solution.py:20
  59.6 0.6 copy-start.5
  59.6 0.8 copy-start.4
  60.4 15.7 %copy-start.8 = (f32[32,2]{0,1:T(2,128)S(1)}, f32[32,2]{0,1:T(2,128)}, u32[]{:S(2)}) copy-start(f32[32,2]{0,1:T(2,128)} %param.35) | copy-start | bytes 772
  69.2 15.1 %copy-start.1 = (f32[32,4,64,64]{3,2,1,0:T(8,128)S(1)}, f32[32,4,64,64]{3,2,1,0:T(8,128)}, u32[]{:S(2)}) copy-start(f32[32,4,64,64]{3,2,1,0:T(8,128)} %param.29) | copy-start | bytes 6291460
  69.2 2.0 %collective-permute-start.18 = (bf16[104,2048]{1,0:T(8,128)(2,1)}, bf16[104,2048]{1,0:T(8,128)(2,1)S(1)}, u32[]{:S(2)}, u32[]{:S(2)}) collective-permute-start(bf16[104,2048]{1,0:T(8,128)(2,1)} %get-tuple-element.7), channel_id=1, source_target_pairs={{0,1},{1,0},{2,3},{3,2},{4,5},{5,4},{6,7},{7,6},{8,9},{9,8},{10,11... | collective-permute-start | bytes 1277960 | tf_op jit(solution)/shard_map/ppermute | solution.py:20
  72.5 6.3 %collective-permute-start.21 = (bf16[18,2048]{1,0:T(8,128)(2,1)S(1)}, bf16[18,2048]{1,0:T(8,128)(2,1)S(1)}, u32[]{:S(2)}, u32[]{:S(2)}) collective-permute-start(bf16[18,2048]{1,0:T(8,128)(2,1)S(1)} %get-tuple-element.17), channel_id=1, source_target_pairs={{0,24},{8,16},{16,8},{24,0},{1,25},{9,17},{17,9},{25,1},{2,26},{10... | collective-permute-start | bytes 221192 | tf_op jit(solution)/shard_map/ppermute | solution.py:20
  74.1 6.3 %collective-permute-start.20 = (bf16[18,2048]{1,0:T(8,128)(2,1)S(1)}, bf16[18,2048]{1,0:T(8,128)(2,1)S(1)}, u32[]{:S(2)}, u32[]{:S(2)}) collective-permute-start(bf16[18,2048]{1,0:T(8,128)(2,1)S(1)} %get-tuple-element.18), channel_id=1, source_target_pairs={{0,16},{8,24},{16,0},{24,8},{1,17},{9,25},{17,1},{25,9},{2,18},{10... | collective-permute-start | bytes 221192 | tf_op jit(solution)/shard_map/ppermute | solution.py:20
  74.6 5.8 %collective-permute-start.19 = (bf16[18,2048]{1,0:T(8,128)(2,1)S(1)}, bf16[18,2048]{1,0:T(8,128)(2,1)S(1)}, u32[]{:S(2)}, u32[]{:S(2)}) collective-permute-start(bf16[18,2048]{1,0:T(8,128)(2,1)S(1)} %get-tuple-element.19), channel_id=1, source_target_pairs={{0,8},{8,0},{16,24},{24,16},{1,9},{9,1},{17,25},{25,17},{2,10},{10... | collective-permute-start | bytes 221192 | tf_op jit(solution)/shard_map/ppermute | solution.py:20
  80.8 6.8 %collective-permute-start.22 = (bf16[32,512]{1,0:T(8,128)(2,1)S(1)}, bf16[32,512]{1,0:T(8,128)(2,1)S(1)}, u32[]{:S(2)}, u32[]{:S(2)}) collective-permute-start(bf16[32,512]{1,0:T(8,128)(2,1)S(1)} %get-tuple-element.29), channel_id=1, source_target_pairs={{0,2},{1,3},{2,0},{3,1},{4,6},{5,7},{6,4},{7,5},{8,10},{9,11},{10,... | collective-permute-start | bytes 98312 | tf_op jit(solution)/shard_map/ppermute | solution.py:20
  80.9 6.8 %collective-permute-start.24 = (bf16[32,512]{1,0:T(8,128)(2,1)S(1)}, bf16[32,512]{1,0:T(8,128)(2,1)S(1)}, u32[]{:S(2)}, u32[]{:S(2)}) collective-permute-start(bf16[32,512]{1,0:T(8,128)(2,1)S(1)} %get-tuple-element.30), channel_id=1, source_target_pairs={{0,6},{1,7},{2,4},{3,5},{4,2},{5,3},{6,0},{7,1},{8,14},{9,15},{10,... | collective-permute-start | bytes 98312 | tf_op jit(solution)/shard_map/ppermute | solution.py:20
  83.2 4.8 %collective-permute-start.23 = (bf16[32,512]{1,0:T(8,128)(2,1)S(1)}, bf16[32,512]{1,0:T(8,128)(2,1)S(1)}, u32[]{:S(2)}, u32[]{:S(2)}) collective-permute-start(bf16[32,512]{1,0:T(8,128)(2,1)S(1)} %get-tuple-element.31), channel_id=1, source_target_pairs={{0,4},{1,5},{2,6},{3,7},{4,0},{5,1},{6,2},{7,3},{8,12},{9,13},{10,... | collective-permute-start | bytes 98312 | tf_op jit(solution)/shard_map/ppermute | solution.py:20
